TPU v7x, 32 devices: a whole 2x2x4 slice. The times are simulated.
32 devices in a mesh: ep: 16 (over z, y, x), tp: 2 (over core).
Axes of the slice: x: 2, y: 2, z: 4, core: 2. Of those that a mesh axis runs over, the one named last changes fastest.
Arguments:
- tokens: bfloat16 [512, 2048], P('ep'), may hold values from -6 to 6
- lru_state: float32 [512, 1024], P('ep', 'tp'), may hold values from -6 to 6
- conv_window: bfloat16 [512, 3, 1024], P('ep', None, 'tp'), may hold values from -6 to 6
- gain_mix_in: float32 [2048], replicated, may hold values from 0.1 to 1.9
- gain_mix_out: float32 [2048], replicated, may hold values from 0.1 to 1.9
- gain_ffn_in: float32 [2048], replicated, may hold values from 0.1 to 1.9
- gain_ffn_out: float32 [2048], replicated, may hold values from 0.1 to 1.9
- w_branch: bfloat16 [2048, 1024], P(None, 'tp'), may hold values from -0.125 to 0.125
- w_input: bfloat16 [2048, 1024], P(None, 'tp'), may hold values from -0.125 to 0.125
- conv_taps: bfloat16 [4, 1024], P(None, 'tp'), may hold values from -3 to 3
- gate_a: bfloat16 [8, 128, 128], P('tp'), may hold values from -0.5 to 0.5
- gate_x: bfloat16 [8, 128, 128], P('tp'), may hold values from -0.5 to 0.5
- decay_rate: float32 [1024], P('tp'), may hold values from 0.001 to 0.3
- w_mix_out: bfloat16 [1024, 2048], P('tp'), may hold values from -0.1875 to 0.1875
- routes: int32 [512, 4], P('ep'), may hold values from 0 to 15, all different within a row; in each aligned block of 32 rows (0 to 31, 32 to 63, ...) at most 16 rows name the same one
- route_weight: float32 [512, 4], P('ep'), may hold values from 0.2 to 1.5
- expert_gate: bfloat16 [16, 2048, 512], P('ep', None, 'tp'), may hold values from -0.125 to 0.125
- expert_up: bfloat16 [16, 2048, 512], P('ep', None, 'tp'), may hold values from -0.125 to 0.125
- expert_down: bfloat16 [16, 512, 2048], P('ep', 'tp'), may hold values from -0.25 to 0.25
- shared_gate: bfloat16 [2048, 512], P(None, 'tp'), may hold values from -0.125 to 0.125
- shared_up: bfloat16 [2048, 512], P(None, 'tp'), may hold values from -0.125 to 0.125
- shared_down: bfloat16 [512, 2048], P('tp'), may hold values from -0.25 to 0.25
Outputs:
- layer_out: bfloat16 [512, 2048], P('ep')
- new_state: float32 [512, 1024], P('ep', 'tp')
- new_window: bfloat16 [512, 3, 1024], P('ep', None, 'tp')
Inputs may be any that keep to these rules, and one draw needn't show every extreme that they name: `routes`: each row names 4 different experts. Within the rows of one device (aligned blocks of 32 rows) no expert is named by more than 16 entries, a bound that some block reaches.
All inputs are finite; a program needn't handle non-finite values.
Results may differ from a plain program's by a relative error of at most 0.014.
Values may be sent and summed in bfloat16 or wider, within the bound.
A program may use at most 64 MiB of HBM per device.

v0:
```python
import jax
import jax.numpy as jnp
from jax import lax
from jax.sharding import PartitionSpec as P


def rms_norm(value, gain):
    return value * lax.rsqrt(jnp.mean(value * value, axis=-1, keepdims=True) + 1e-06) * gain


def rounded_term(value):
    return lax.optimization_barrier(value.astype(jnp.bfloat16)).astype(jnp.float32)


def on_device(
    tokens,
    lru_state,
    conv_window,
    gain_mix_in,
    gain_mix_out,
    gain_ffn_in,
    gain_ffn_out,
    w_branch,
    w_input,
    conv_taps,
    gate_a,
    gate_x,
    decay_rate,
    w_mix_out,
    routes,
    route_weight,
    expert_gate,
    expert_up,
    expert_down,
    shared_gate,
    shared_up,
    shared_down,
):
    resid = tokens.astype(jnp.float32)
    normed = rms_norm(resid, gain_mix_in).astype(jnp.bfloat16)
    branch = jnp.dot(normed, w_branch, preferred_element_type=jnp.float32)
    inflow = jnp.dot(normed, w_input, preferred_element_type=jnp.float32).astype(jnp.bfloat16)
    window = jnp.concatenate([conv_window, inflow[:, None, :]], axis=1)
    new_window = window[:, 1:]
    conv = jnp.sum(window.astype(jnp.float32) * conv_taps.astype(jnp.float32)[None], axis=1)
    count, local_ch = conv.shape
    groups, group_dim = (gate_a.shape[0], gate_a.shape[1])
    grouped = conv.astype(jnp.bfloat16).reshape(count, groups, group_dim)
    recur_gate = jax.nn.sigmoid(
        jnp.einsum("sbi,bij->sbj", grouped, gate_a, preferred_element_type=jnp.float32).reshape(
            count, local_ch
        )
    )
    input_gate = jax.nn.sigmoid(
        jnp.einsum("sbi,bij->sbj", grouped, gate_x, preferred_element_type=jnp.float32).reshape(
            count, local_ch
        )
    )
    log_decay = -8.0 * recur_gate * decay_rate[None]
    new_state = (
        jnp.exp(log_decay) * lru_state + jnp.sqrt(-jnp.expm1(2.0 * log_decay)) * conv * input_gate
    )
    gated = (new_state * jax.nn.gelu(branch)).astype(jnp.bfloat16)
    mix_term = rounded_term(jnp.dot(gated, w_mix_out, preferred_element_type=jnp.float32))
    mixed = lax.psum(mix_term.astype(jnp.bfloat16), "tp").astype(jnp.float32)
    middle = (resid + rms_norm(mixed, gain_mix_out)).astype(jnp.bfloat16)
    ffn_in = rms_norm(middle.astype(jnp.float32), gain_ffn_in).astype(jnp.bfloat16)
    width = ffn_in.shape[1]
    top = routes.shape[1]
    local_exp = expert_gate.shape[0]
    experts = local_exp * lax.axis_size("ep")
    capacity = max(2, 2 * count * top // experts)
    flat = routes.reshape(count * top)
    onehot = (flat[:, None] == jnp.arange(experts, dtype=jnp.int32)[None, :]).astype(jnp.int32)
    rank = jnp.sum(onehot * (jnp.cumsum(onehot, axis=0) - 1), axis=-1)
    dest = flat * capacity + rank
    slot_ids = jnp.arange(experts * capacity, dtype=jnp.int32)
    placed = jnp.any(dest.reshape(count, top)[None, :, :] == slot_ids[:, None, None], axis=-1)
    outbound = jnp.dot(placed.astype(jnp.bfloat16), ffn_in, preferred_element_type=jnp.float32)
    outbound = outbound.astype(jnp.bfloat16).reshape(experts, capacity, width)
    shared_hidden = (
        jax.nn.silu(jnp.dot(ffn_in, shared_gate, preferred_element_type=jnp.float32))
        * jnp.dot(ffn_in, shared_up, preferred_element_type=jnp.float32)
    ).astype(jnp.bfloat16)
    shared = lax.psum(
        rounded_term(
            jnp.dot(shared_hidden, shared_down, preferred_element_type=jnp.float32)
        ).astype(jnp.bfloat16),
        "tp",
    ).astype(jnp.float32)
    share = width // lax.axis_size("tp")
    own = lax.dynamic_slice_in_dim(outbound, lax.axis_index("tp") * share, share, 2)
    arrived = lax.all_to_all(own, "ep", split_axis=0, concat_axis=1, tiled=True)
    rows = lax.all_gather(arrived, "tp", axis=2, tiled=True)
    hidden = (
        jax.nn.silu(
            jnp.einsum("erd,edf->erf", rows, expert_gate, preferred_element_type=jnp.float32)
        )
        * jnp.einsum("erd,edf->erf", rows, expert_up, preferred_element_type=jnp.float32)
    ).astype(jnp.bfloat16)
    summed = lax.psum_scatter(
        rounded_term(
            jnp.einsum("erf,efd->erd", hidden, expert_down, preferred_element_type=jnp.float32)
        ).astype(jnp.bfloat16),
        "tp",
        scatter_dimension=2,
        tiled=True,
    )
    back = lax.all_to_all(summed, "ep", split_axis=1, concat_axis=0, tiled=True)
    flat_out = back.reshape(experts * capacity, share)
    picked = flat_out[dest].reshape(count, top, flat_out.shape[1])
    routed_share = jnp.sum(picked.astype(jnp.float32) * route_weight[:, :, None], axis=1).astype(
        jnp.bfloat16
    )
    routed = lax.all_gather(routed_share, "tp", axis=1, tiled=True)
    total = routed.astype(jnp.float32) + shared
    layer_out = (middle.astype(jnp.float32) + rms_norm(total, gain_ffn_out)).astype(jnp.bfloat16)
    return (layer_out, new_state, new_window)


def solution(mesh):
    placed = (
        P("ep", None),
        P("ep", "tp"),
        P("ep", None, "tp"),
        P(),
        P(),
        P(),
        P(),
        P(None, "tp"),
        P(None, "tp"),
        P(None, "tp"),
        P("tp", None, None),
        P("tp", None, None),
        P("tp"),
        P("tp", None),
        P("ep", None),
        P("ep", None),
        P("ep", None, "tp"),
        P("ep", None, "tp"),
        P("ep", "tp", None),
        P(None, "tp"),
        P(None, "tp"),
        P("tp", None),
    )
    return jax.shard_map(
        on_device,
        mesh=mesh,
        in_specs=placed,
        out_specs=(P("ep", None), P("ep", "tp"), P("ep", None, "tp")),
        check_vma=False,
    )
```

profile of v0, /device:TPU:0, one launch (start us, length us, event | category | flops | bytes accessed | tf_op | source)
XLA Modules:
  0.0 134.1 jit_solution(11292914418998984690)
XLA Ops:
  7.3 1.2 fusion.24
  8.5 0.7 convert_element_type.92
  9.2 2.2 %fusion.10 = bf16[32,1,512]{2,0,1:T(8,128)(2,1)S(1)} fusion(bf16[2048,512]{1,0:T(8,128)(2,1)} %param.30, bf16[32,2048]{1,0:T(8,128)(2,1)} %param.22, f32[2048]{0:T(1024)} %param.25, f32[32]{0:T(128)S(1)} %add_rsqrt_fusion.3), kind=kOutput, calls=%fused_computation.19 | convolution fusion | flops 67387392 | bytes 2269312 | tf_op jit(solution)/shard_map/dot_general | solution.py:42
  12.0 3.2 %convolution_convert_fusion.3 = bf16[32,2048]{1,0:T(8,128)(2,1)} fusion(bf16[512,2048]{1,0:T(8,128)(2,1)S(1)} %copy-done, f32[32,512]{1,0:T(8,128)S(1)} %fusion.49, bf16[2048,512]{1,0:T(8,128)(2,1)} %param.29, bf16[32,2048]{1,0:T(8,128)(2,1)S(1)} %copy-done.2, f32[2048]{0:T(1024)S(1)} %copy-done.10, f32[32]{0:T(128)S(1)} %add_rsqrt_fusion.3), kind=kOutput, calls=%fused_computation.5 | convolution fusion | flops 134709248 | bytes 4530304 | tf_op jit(solution)/shard_map/dot_general | solution.py:64
  16.1 0.6 broadcast_multiply_fusion
  16.9 19.2 %all-reduce.3.cloned.1.call-done = bf16[32,2048]{1,0:T(8,128)(2,1)} async-done(((bf16[32,2048]{1,0:T(8,128)(2,1)}), bf16[32,2048]{1,0:T(8,128)(2,1)}) %all-reduce.3.cloned.1.call-update) | async-done | bytes 131088 | tf_op jit(solution)/shard_map/psum | solution.py:65
  36.1 1.0 fusion.22
  37.1 1.1 fusion.28
  38.3 0.5 convolution_convert_fusion.1
  38.9 22.2 %all_to_all.21 = bf16[16,16,1024]{2,1,0:T(8,128)(2,1)} all-to-all(bf16[16,16,1024]{2,1,0:T(8,128)(2,1)S(1)} %constant_dynamic-slice_fusion), channel_id=1, replica_groups=mesh['ep'=16,'tp'=2] {'ep'}, dimensions={0} | all-to-all | bytes 1048576 | tf_op jit(solution)/shard_map/all_to_all | solution.py:93
  61.1 7.5 %all-gather.2.cloned.1.call-done = bf16[1,256,2048]{2,1,0:T(8,128)(2,1)} async-done(((bf16[1,256,1024]{2,1,0:T(8,128)(2,1)}), bf16[1,256,2048]{2,1,0:T(8,128)(2,1)}) %all-gather.2.cloned.1.call-update) | async-done | bytes 1048592 | tf_op jit(solution)/shard_map/all_gather | solution.py:94
  68.6 2.1 %fusion.14 = f32[256,256]{1,0:T(8,128)S(1)} fusion(bf16[1,2048,256]{2,1,0:T(8,128)(2,1)} %param.38, bf16[1,256,2048]{2,1,0:T(8,128)(2,1)} %all-gather.2.cloned.1.call-done), kind=kOutput, calls=%fused_computation.24 | convolution fusion | flops 268435456 | bytes 2359296 | tf_op jit(solution)/shard_map/erd,edf->erf/dot_general | solution.py:97
  70.7 3.8 %fusion = bf16[1,256,2048]{2,1,0:T(8,128)(2,1)} fusion(bf16[1,256,2048]{2,1,0:T(8,128)(2,1)} %param.40, bf16[1,2048,256]{2,1,0:T(8,128)(2,1)} %param.39, bf16[1,256,2048]{2,1,0:T(8,128)(2,1)S(1)} %copy-done.1, f32[256,256]{1,0:T(8,128)S(1)} %fusion.14), kind=kOutput, calls=%fused_computation.3 | convolution fusion | flops 537788416 | bytes 4456448 | tf_op jit(solution)/shard_map/erf,efd->erd/dot_general | solution.py:103
  74.6 0.8 mul.225
  75.4 0.8 copy.61
  76.2 8.1 %reduce-scatter.2.cloned.1.call-done = bf16[1,256,1024]{2,1,0:T(8,128)(2,1)} async-done(((bf16[1,256,2048]{2,1,0:T(8,128)(2,1)}), bf16[1,256,1024]{2,1,0:T(8,128)(2,1)}) %reduce-scatter.2.cloned.1.call-update) | async-done | bytes 524304 | tf_op jit(solution)/shard_map/reduce_scatter | solution.py:101
  84.3 1.9 %copy.81 = bf16[1,256,1024]{2,0,1:T(2,128)(2,1)S(1)} copy(bf16[1,256,1024]{2,1,0:T(8,128)(2,1)} %reduce-scatter.2.cloned.1.call-done) | data formatting | bytes 1048576 | tf_op jit(solution)/shard_map/reduce_scatter | solution.py:101
  86.2 0.5 broadcast.143
  86.7 4.5 %reduce = bf16[256,1024]{1,0:T(8,128)(2,1)} reduce(bf16[256,1,1024]{2,1,0:T(2,128)(2,1)S(1)} %bitcast.73, bf16[]{:T(256)} %broadcast.143), dimensions={1}, to_apply=%bitcast.70.reduce_sub_computation | reduce | bytes 1048578
  91.2 2.2 %reshape.155 = bf16[16,2,8192]{2,1,0:T(2,128)(2,1)} reshape(bf16[256,1024]{1,0:T(8,128)(2,1)} %reduce) | data formatting | bytes 1048576
  93.4 6.8 %all-to-all-start.1 = ((bf16[16,2,8192]{2,1,0:T(2,128)(2,1)}), bf16[16,2,8192]{2,1,0:T(2,128)(2,1)S(1)}, u32[]{:S(2)}, u32[]{:S(2)}) async-start(bf16[16,2,8192]{2,1,0:T(2,128)(2,1)} %reshape.155), calls=%async_computation.2 | async-start | bytes 1048576 | tf_op jit(solution)/shard_map/all_to_all | solution.py:109
  100.3 0.7 fusion.39
  100.9 1.5 %fusion.82 = f32[32,256]{1,0:T(8,128)S(1)} fusion(bf16[2048,256]{1,0:T(8,128)(2,1)} %param.41, bf16[32,2048]{1,0:T(8,128)(2,1)S(1)} %get-tuple-element.4, f32[2048]{0:T(1024)S(1)} %copy-done.8, f32[32]{0:T(128)S(1)} %add_rsqrt_fusion.1), kind=kOutput, calls=%fused_computation.113 | convolution fusion | flops 33816576 | bytes 1220736 | tf_op jit(solution)/shard_map/dot_general | solution.py:82
  102.5 3.0 %convolution_convert_fusion.2 = bf16[32,2048]{1,0:T(8,128)(2,1)} fusion(bf16[256,2048]{1,0:T(8,128)(2,1)} %param.43, bf16[2048,256]{1,0:T(8,128)(2,1)} %param.42, f32[32,256]{1,0:T(8,128)S(1)} %fusion.82, bf16[32,2048]{1,0:T(8,128)(2,1)S(1)} %get-tuple-element.4, f32[2048]{0:T(1024)S(1)} %copy-done.8, f32[32]{0:T(128)S(1)} %add_rsqrt_fusion.1), kind=kOutput, calls=%fused_computation.4 | convolution fusion | flops 67485696 | bytes 2400384 | tf_op jit(solution)/shard_map/dot_general | solution.py:87
  105.5 10.2 %all-to-all-done.1 = bf16[16,2,8192]{2,1,0:T(2,128)(2,1)S(1)} async-done(((bf16[16,2,8192]{2,1,0:T(2,128)(2,1)}), bf16[16,2,8192]{2,1,0:T(2,128)(2,1)S(1)}, u32[]{:S(2)}, u32[]{:S(2)}) %all-to-all-start.1) | async-done | bytes 524320 | tf_op jit(solution)/shard_map/all_to_all | solution.py:109
  115.7 1.8 %reshape.156 = bf16[256,1,1024]{2,1,0:T(2,128)(2,1)} reshape(bf16[16,2,8192]{2,1,0:T(2,128)(2,1)S(1)} %all-to-all-done.1) | data formatting | bytes 1048576
  117.4 1.4 %copy.80 = bf16[1,256,1024]{2,1,0:T(8,128)(2,1)S(1)} copy(bf16[1,256,1024]{2,0,1:T(2,128)(2,1)} %bitcast.72) | data formatting | bytes 1048576
  118.9 0.9 gather_fusion
  120.3 1.9 %all_gather.7 = bf16[32,2048]{1,0:T(8,128)(2,1)S(1)} all-gather(bf16[32,1024]{1,0:T(8,128)(2,1)S(1)} %multiply_reduce_fusion), channel_id=1, replica_groups=mesh['ep'=16,'tp'=2] {'tp'}, dimensions={1}, use_global_device_ids=true | all-gather | bytes 196608 | tf_op jit(solution)/shard_map/all_gather | solution.py:115
  122.2 2.7 %all-reduce.5.cloned.1.call-done = bf16[32,2048]{1,0:T(8,128)(2,1)} async-done(((bf16[32,2048]{1,0:T(8,128)(2,1)}), bf16[32,2048]{1,0:T(8,128)(2,1)}) %all-reduce.5.cloned.1.call-update) | async-done | bytes 131088 | tf_op jit(solution)/shard_map/psum | solution.py:85
  124.8 1.1 multiply_reduce_fusion.1
  125.9 1.7 %fusion.31 = bf16[32,2048]{1,0:T(8,128)(2,1)} fusion(bf16[32,2048]{1,0:T(8,128)(2,1)S(1)} %get-tuple-element.4, bf16[32,2048]{1,0:T(8,128)(2,1)} %all-reduce.5.cloned.1.call-done, bf16[32,2048]{1,0:T(8,128)(2,1)S(1)} %all_gather.7, f32[2048]{0:T(1024)S(1)} %copy-done.11, f32[32]{0:T(128)S(1)} %add_rsqrt_fusion), kind=kLoop, calls=%fused_computation.47 | loop fusion | flops 524288 | bytes 532608 | tf_op jit(solution)/shard_map/convert_element_type | solution.py:117
  (64 shorter events, 2.3 us)
Async XLA Ops:
  7.2 4.8 %copy-start = (bf16[512,2048]{1,0:T(8,128)(2,1)S(1)}, bf16[512,2048]{1,0:T(8,128)(2,1)}, u32[]{:S(2)}) copy-start(bf16[512,2048]{1,0:T(8,128)(2,1)} %param.35) | copy-start | bytes 6291460
  7.2 4.8 %copy-start.2 = (bf16[32,2048]{1,0:T(8,128)(2,1)S(1)}, bf16[32,2048]{1,0:T(8,128)(2,1)}, u32[]{:S(2)}) copy-start(bf16[32,2048]{1,0:T(8,128)(2,1)} %param.22) | copy-start | bytes 393220
  7.2 4.8 %copy-start.10 = (f32[2048]{0:T(1024)S(1)}, f32[2048]{0:T(1024)}, u32[]{:S(2)}) copy-start(f32[2048]{0:T(1024)} %param.25) | copy-start | bytes 24580
  7.2 4.2 %copy-start.3 = (bf16[32,3,512]{2,0,1:T(8,128)(2,1)S(1)}, bf16[32,3,512]{2,0,1:T(8,128)(2,1)}, u32[]{:S(2)}) copy-start(bf16[32,3,512]{2,0,1:T(8,128)(2,1)} %param.24) | copy-start | bytes 294916
  7.2 4.2 %copy-start.15 = (bf16[4,128,128]{2,1,0:T(8,128)(2,1)S(1)}, bf16[4,128,128]{2,1,0:T(8,128)(2,1)}, u32[]{:S(2)}) copy-start(bf16[4,128,128]{2,1,0:T(8,128)(2,1)} %param.33) | copy-start | bytes 393220
  7.2 4.4 %copy-start.16 = (bf16[4,128,128]{2,1,0:T(8,128)(2,1)S(1)}, bf16[4,128,128]{2,1,0:T(8,128)(2,1)}, u32[]{:S(2)}) copy-start(bf16[4,128,128]{2,1,0:T(8,128)(2,1)} %param.32) | copy-start | bytes 393220
  7.2 4.6 %copy-start.14 = (f32[512]{0:T(512)S(1)}, f32[512]{0:T(512)}, u32[]{:S(2)}) copy-start(f32[512]{0:T(512)} %param.34) | copy-start | bytes 6148
  7.2 4.6 %copy-start.9 = (f32[32,512]{1,0:T(8,128)S(1)}, f32[32,512]{1,0:T(8,128)}, u32[]{:S(2)}) copy-start(f32[32,512]{1,0:T(8,128)} %param.23) | copy-start | bytes 196612
  7.3 28.8 %all-reduce.3.cloned.1.call-start = ((), (), s32[]{:S(2)}) async-start(), calls=%async_computation.3 | async-start | bytes 262144 | tf_op jit(solution)/shard_map/psum | solution.py:65
  11.4 3.8 %copy-start.5 = (bf16[32,1,512]{2,0,1:T(8,128)(2,1)}, bf16[32,1,512]{2,0,1:T(8,128)(2,1)S(1)}, u32[]{:S(2)}) copy-start(bf16[32,1,512]{2,0,1:T(8,128)(2,1)S(1)} %fusion.10) | copy-start | bytes 98308
  12.0 3.3 %copy-start.7 = (f32[32,512]{1,0:T(8,128)}, f32[32,512]{1,0:T(8,128)S(1)}, u32[]{:S(2)}) copy-start(f32[32,512]{1,0:T(8,128)S(1)} %fusion.49) | copy-start | bytes 196612
  12.0 3.4 %copy-start.13 = (s32[32,4]{0,1:T(4,128)S(1)}, s32[32,4]{0,1:T(4,128)}, u32[]{:S(2)}) copy-start(s32[32,4]{0,1:T(4,128)} %param.36) | copy-start | bytes 1540
  12.0 25.1 %copy-start.12 = (f32[2048]{0:T(1024)S(1)}, f32[2048]{0:T(1024)}, u32[]{:S(2)}) copy-start(f32[2048]{0:T(1024)} %param.26) | copy-start | bytes 24580
  12.0 26.3 %copy-start.8 = (f32[2048]{0:T(1024)S(1)}, f32[2048]{0:T(1024)}, u32[]{:S(2)}) copy-start(f32[2048]{0:T(1024)} %param.27) | copy-start | bytes 24580
  15.3 53.4 %all-gather.2.cloned.1.call-start = ((), (), s32[]{:S(2)}) async-start(), calls=%async_computation.4 | async-start | bytes 1572864 | tf_op jit(solution)/shard_map/all_gather | solution.py:94
  61.1 23.2 %reduce-scatter.2.cloned.1.call-start = ((), (), s32[]{:S(2)}) async-start(), calls=%async_computation.5 | async-start | bytes 1572864 | tf_op jit(solution)/shard_map/reduce_scatter | solution.py:101
  68.6 2.1 %copy-start.1 = (bf16[1,256,2048]{2,1,0:T(8,128)(2,1)S(1)}, bf16[1,256,2048]{2,1,0:T(8,128)(2,1)}, u32[]{:S(2)}) copy-start(bf16[1,256,2048]{2,1,0:T(8,128)(2,1)} %all-gather.2.cloned.1.call-done) | copy-start | bytes 3145732
  86.1 14.1 %copy-start.4 = (bf16[32,3,512]{2,0,1:T(8,128)(2,1)S(1)}, bf16[32,3,512]{2,0,1:T(8,128)(2,1)}, u32[]{:S(2)}) copy-start(bf16[32,3,512]{2,0,1:T(8,128)(2,1)} %param.24) | copy-start | bytes 294916
  86.2 14.1 %copy-start.6 = (bf16[32,1,512]{2,0,1:T(8,128)(2,1)S(1)}, bf16[32,1,512]{2,0,1:T(8,128)(2,1)}, u32[]{:S(2)}) copy-start(bf16[32,1,512]{2,0,1:T(8,128)(2,1)} %copy-done.5) | copy-start | bytes 98308
  93.4 22.3 %all-to-all-start.1 = ((bf16[16,2,8192]{2,1,0:T(2,128)(2,1)}), bf16[16,2,8192]{2,1,0:T(2,128)(2,1)S(1)}, u32[]{:S(2)}, u32[]{:S(2)}) async-start(bf16[16,2,8192]{2,1,0:T(2,128)(2,1)} %reshape.155), calls=%async_computation.2 | async-start | bytes 1048576 | tf_op jit(solution)/shard_map/all_to_all | solution.py:109
  100.2 24.7 %all-reduce.5.cloned.1.call-start = ((), (), s32[]{:S(2)}) async-start(), calls=%async_computation.6 | async-start | bytes 262144 | tf_op jit(solution)/shard_map/psum | solution.py:85
  118.8 7.1 %copy-start.11 = (f32[2048]{0:T(1024)S(1)}, f32[2048]{0:T(1024)}, u32[]{:S(2)}) copy-start(f32[2048]{0:T(1024)} %param.28) | copy-start | bytes 24580
Sparse Core Ops, SparseCore 0:
  15.4 20.6 all-reduce.2
  61.2 7.3 all-gather.1
  74.7 9.5 reduce-scatter.1
  105.6 19.1 all-reduce.4
where the time goes:
time: 135 us; the launch traced here: 134 us
  waiting for transfers between devices  47.7 us (35%)
  blocking collectives  24.1 us (18%)
  matrix products  16.7 us (12%)
  between operations  14.2 us (11%)
  other arithmetic  13.6 us (10%)
  local copies, waits for them, and re-layouts  10.9 us (8%)
  starting transfers between devices  6.93 us (5%)
    all_to_all x1, blocking collectives, on_device(): arrived = lax.all_to_all(own, 'ep', split_axis=0, concat_axis=1, tiled=True)  22.2 us
    psum x1, waiting for transfers between devices, on_device(): mixed = lax.psum(mix_term.astype(jnp.bfloat16), 'tp').astype(jnp.float32)  19.2 us
    all_to_all x1, waiting for transfers between devices, on_device(): back = lax.all_to_all(summed, 'ep', split_axis=1, concat_axis=0, tiled=True)  10.2 us
    reduce_scatter x1, waiting for transfers between devices, on_device(): lax.psum_scatter(rounded_term(jnp.einsum('erf,efd->erd', hidden, expert_d...  8.14 us
    all_gather x1, waiting for transfers between devices, on_device(): rows = lax.all_gather(arrived, 'tp', axis=2, tiled=True)  7.49 us
    unnamed x40, local copies, waits for them, and re-layouts  6.86 us
    all_to_all x1, starting transfers between devices, on_device(): back = lax.all_to_all(summed, 'ep', split_axis=1, concat_axis=0, tiled=True)  6.77 us
    unnamed x1, other arithmetic  4.5 us
  transfers between devices with their start and end apart: 5, of which 5 were waited for; matrix products, arithmetic and copies ran while one was open for 10% of the time, Pallas kernels for 0%

commit v1 on v0

--- a/solution.py
+++ b/solution.py
@@ -62,7 +62,7 @@
     )
     gated = (new_state * jax.nn.gelu(branch)).astype(jnp.bfloat16)
     mix_term = rounded_term(jnp.dot(gated, w_mix_out, preferred_element_type=jnp.float32))
-    mixed = lax.psum(mix_term.astype(jnp.bfloat16), "tp").astype(jnp.float32)
+    mixed = jnp.sum(lax.all_gather(mix_term.astype(jnp.bfloat16), "tp"), axis=0).astype(jnp.float32)
     middle = (resid + rms_norm(mixed, gain_mix_out)).astype(jnp.bfloat16)
     ffn_in = rms_norm(middle.astype(jnp.float32), gain_ffn_in).astype(jnp.bfloat16)
     width = ffn_in.shape[1]

time: 135 us -> 116 us (0.86)
  waiting for transfers between devices: 47.7 us -> 29.1 us
  blocking collectives: 24.1 us -> 27.5 us
  other arithmetic: 13.6 us -> 11.9 us
    psum x1 -> x0, waiting for transfers between devices: 19.2 us -> none  [on_device(): mixed = lax.psum(mix_term.astype(jnp.bfloat16), 'tp').astype(jnp.float32)]
    all_gather x0 -> x1, blocking collectives: none -> 2.12 us  [on_device(): lax.all_gather(mix_term.astype(jnp.bfloat16), 'tp')]
    reduce_sum x4, other arithmetic: 4.42 us -> 2.62 us  [rms_norm(): jnp.mean(value * value, axis=-1, keepdims=True) + 1e-06]
    reduce_scatter x1, waiting for transfers between devices: 8.14 us -> 9.7 us  [on_device(): lax.psum_scatter(rounded_term(jnp.einsum('erf,efd->erd', hidden, expert_d...]
    unnamed x40 -> x44, local copies, waits for them, and re-layouts: 6.86 us -> 6.37 us
  transfers between devices with their start and end apart: 5 -> 4, of which waited for: 5 -> 4; matrix products, arithmetic and copies ran while one was open for 10% -> 9% of each run, Pallas kernels for 0% -> 0%
where the time goes in v1:
time: 116 us; the launch traced here: 115 us
  waiting for transfers between devices  29.1 us (25%)
  blocking collectives  27.5 us (24%)
  matrix products  16 us (14%)
  between operations  14.2 us (12%)
  other arithmetic  11.9 us (10%)
  local copies, waits for them, and re-layouts  9.69 us (8%)
  starting transfers between devices  6.92 us (6%)
    all_to_all x1, blocking collectives, on_device(): arrived = lax.all_to_all(own, 'ep', split_axis=0, concat_axis=1, tiled=True)  23.5 us
    all_to_all x1, waiting for transfers between devices, on_device(): back = lax.all_to_all(summed, 'ep', split_axis=1, concat_axis=0, tiled=True)  9.93 us
    reduce_scatter x1, waiting for transfers between devices, on_device(): lax.psum_scatter(rounded_term(jnp.einsum('erf,efd->erd', hidden, expert_d...  9.7 us
    all_gather x1, waiting for transfers between devices, on_device(): rows = lax.all_gather(arrived, 'tp', axis=2, tiled=True)  7.46 us
    all_to_all x1, starting transfers between devices, on_device(): back = lax.all_to_all(summed, 'ep', split_axis=1, concat_axis=0, tiled=True)  6.79 us
    unnamed x44, local copies, waits for them, and re-layouts  6.37 us
    unnamed x1, other arithmetic  4.5 us
    dot_general x1, matrix products, on_device(): jnp.einsum('erf,efd->erd', hidden, expert_down, preferred_element_type=jn...  3.82 us
  transfers between devices with their start and end apart: 4, of which 4 were waited for; matrix products, arithmetic and copies ran while one was open for 9% of the time, Pallas kernels for 0%

profile of v1, /device:TPU:0, one launch (start us, length us, event | category | flops | bytes accessed | tf_op | source)
XLA Modules:
  0.0 115.3 jit_solution(774264285441566568)
XLA Ops:
  7.3 1.2 %fusion.24 = f32[32]{0:T(128)S(1)} fusion(bf16[32,2048]{1,0:T(8,128)(2,1)} %param.22), kind=kLoop, calls=%fused_computation.40 | loop fusion | flops 196576 | bytes 131200 | tf_op jit(solution)/shard_map/reduce_sum | solution.py:8
  8.5 0.7 convert_element_type.94
  9.2 2.2 %fusion.10 = bf16[32,1,512]{2,0,1:T(8,128)(2,1)S(1)} fusion(bf16[2048,512]{1,0:T(8,128)(2,1)} %param.30, bf16[32,2048]{1,0:T(8,128)(2,1)} %param.22, f32[2048]{0:T(1024)} %param.25, f32[32]{0:T(128)S(1)} %add_rsqrt_fusion.3), kind=kOutput, calls=%fused_computation.19 | convolution fusion | flops 67387392 | bytes 2269312 | tf_op jit(solution)/shard_map/dot_general | solution.py:42
  11.8 0.2 copy-done.5
  12.2 2.6 %convolution_convert_fusion.3 = bf16[32,2048]{1,0:T(8,128)(2,1)S(1)} fusion(bf16[512,2048]{1,0:T(8,128)(2,1)S(1)} %copy-done, f32[32,512]{1,0:T(8,128)S(1)} %fusion.49, bf16[2048,512]{1,0:T(8,128)(2,1)} %param.29, bf16[32,2048]{1,0:T(8,128)(2,1)S(1)} %copy-done.2, f32[2048]{0:T(1024)S(1)} %copy-done.11, f32[32]{0:T(128)S(1)} %add_rsqrt_fusion.3), kind=kOutput, calls=%fused_computation.5 | convolution fusion | flops 134709248 | bytes 4530304 | tf_op jit(solution)/shard_map/dot_general | solution.py:64
  14.8 2.1 %all-gather = bf16[64,2048]{1,0:T(8,128)(2,1)S(1)} all-gather(bf16[32,2048]{1,0:T(8,128)(2,1)S(1)} %convolution_convert_fusion.3), channel_id=2, replica_groups=mesh['ep'=16,'tp'=2] {'tp'}, dimensions={0}, use_global_device_ids=true | all-gather | bytes 393216 | tf_op jit(solution)/shard_map/all_gather | solution.py:65
  17.1 0.2 fusion.28
  18.1 0.6 broadcast_multiply_fusion
  18.9 0.5 convolution_convert_fusion.1
  19.5 23.5 %all_to_all.21 = bf16[16,16,1024]{2,1,0:T(8,128)(2,1)} all-to-all(bf16[16,16,1024]{2,1,0:T(8,128)(2,1)S(1)} %constant_dynamic-slice_fusion), channel_id=1, replica_groups=mesh['ep'=16,'tp'=2] {'ep'}, dimensions={0} | all-to-all | bytes 1048576 | tf_op jit(solution)/shard_map/all_to_all | solution.py:93
  43.1 7.5 %all-gather.3.cloned.1.call-done = bf16[1,256,2048]{2,1,0:T(8,128)(2,1)} async-done(((bf16[1,256,1024]{2,1,0:T(8,128)(2,1)}), bf16[1,256,2048]{2,1,0:T(8,128)(2,1)}) %all-gather.3.cloned.1.call-update) | async-done | bytes 1048592 | tf_op jit(solution)/shard_map/all_gather | solution.py:94
  50.5 2.1 %fusion.14 = f32[256,256]{1,0:T(8,128)S(1)} fusion(bf16[1,2048,256]{2,1,0:T(8,128)(2,1)} %param.38, bf16[1,256,2048]{2,1,0:T(8,128)(2,1)} %all-gather.3.cloned.1.call-done), kind=kOutput, calls=%fused_computation.24 | convolution fusion | flops 268435456 | bytes 2359296 | tf_op jit(solution)/shard_map/erd,edf->erf/dot_general | solution.py:97
  52.6 3.8 %fusion = bf16[1,256,2048]{2,1,0:T(8,128)(2,1)} fusion(bf16[1,256,2048]{2,1,0:T(8,128)(2,1)} %param.40, bf16[1,2048,256]{2,1,0:T(8,128)(2,1)} %param.39, bf16[1,256,2048]{2,1,0:T(8,128)(2,1)S(1)} %copy-done.1, f32[256,256]{1,0:T(8,128)S(1)} %fusion.14), kind=kOutput, calls=%fused_computation.3 | convolution fusion | flops 537788416 | bytes 4456448 | tf_op jit(solution)/shard_map/erf,efd->erd/dot_general | solution.py:103
  56.5 9.7 %reduce-scatter.2.cloned.1.call-done = bf16[1,256,1024]{2,1,0:T(8,128)(2,1)} async-done(((bf16[1,256,2048]{2,1,0:T(8,128)(2,1)}), bf16[1,256,1024]{2,1,0:T(8,128)(2,1)}) %reduce-scatter.2.cloned.1.call-update) | async-done | bytes 524304 | tf_op jit(solution)/shard_map/reduce_scatter | solution.py:101
  66.2 1.9 %copy.81 = bf16[1,256,1024]{2,0,1:T(2,128)(2,1)S(1)} copy(bf16[1,256,1024]{2,1,0:T(8,128)(2,1)} %reduce-scatter.2.cloned.1.call-done) | data formatting | bytes 1048576 | tf_op jit(solution)/shard_map/reduce_scatter | solution.py:101
  68.0 0.5 broadcast.143
  68.5 4.5 %reduce.1 = bf16[256,1024]{1,0:T(8,128)(2,1)} reduce(bf16[256,1,1024]{2,1,0:T(2,128)(2,1)S(1)} %bitcast.74, bf16[]{:T(256)} %broadcast.143), dimensions={1}, to_apply=%bitcast.71.reduce_sub_computation | reduce | bytes 1048578
  73.0 2.2 %reshape.156 = bf16[16,2,8192]{2,1,0:T(2,128)(2,1)} reshape(bf16[256,1024]{1,0:T(8,128)(2,1)} %reduce.1) | data formatting | bytes 1048576
  75.2 6.8 %all-to-all-start.1 = ((bf16[16,2,8192]{2,1,0:T(2,128)(2,1)}), bf16[16,2,8192]{2,1,0:T(2,128)(2,1)S(1)}, u32[]{:S(2)}, u32[]{:S(2)}) async-start(bf16[16,2,8192]{2,1,0:T(2,128)(2,1)} %reshape.156), calls=%async_computation.2 | async-start | bytes 1048576 | tf_op jit(solution)/shard_map/all_to_all | solution.py:109
  82.1 1.5 %fusion.82 = f32[32,256]{1,0:T(8,128)S(1)} fusion(bf16[2048,256]{1,0:T(8,128)(2,1)} %param.41, bf16[32,2048]{1,0:T(8,128)(2,1)S(1)} %get-tuple-element.4, f32[2048]{0:T(1024)S(1)} %copy-done.8, f32[32]{0:T(128)S(1)} %add_rsqrt_fusion.1), kind=kOutput, calls=%fused_computation.113 | convolution fusion | flops 33816576 | bytes 1220736 | tf_op jit(solution)/shard_map/dot_general | solution.py:82
  83.7 3.0 %convolution_convert_fusion.2 = bf16[32,2048]{1,0:T(8,128)(2,1)} fusion(bf16[256,2048]{1,0:T(8,128)(2,1)} %param.43, bf16[2048,256]{1,0:T(8,128)(2,1)} %param.42, f32[32,256]{1,0:T(8,128)S(1)} %fusion.82, bf16[32,2048]{1,0:T(8,128)(2,1)S(1)} %get-tuple-element.4, f32[2048]{0:T(1024)S(1)} %copy-done.8, f32[32]{0:T(128)S(1)} %add_rsqrt_fusion.1), kind=kOutput, calls=%fused_computation.4 | convolution fusion | flops 67485696 | bytes 2400384 | tf_op jit(solution)/shard_map/dot_general | solution.py:87
  86.9 0.7 fusion.39
  87.6 9.9 %all-to-all-done.1 = bf16[16,2,8192]{2,1,0:T(2,128)(2,1)S(1)} async-done(((bf16[16,2,8192]{2,1,0:T(2,128)(2,1)}), bf16[16,2,8192]{2,1,0:T(2,128)(2,1)S(1)}, u32[]{:S(2)}, u32[]{:S(2)}) %all-to-all-start.1) | async-done | bytes 524320 | tf_op jit(solution)/shard_map/all_to_all | solution.py:109
  97.5 1.8 %reshape.157 = bf16[256,1,1024]{2,1,0:T(2,128)(2,1)} reshape(bf16[16,2,8192]{2,1,0:T(2,128)(2,1)S(1)} %all-to-all-done.1) | data formatting | bytes 1048576
  99.3 1.4 %copy.80 = bf16[1,256,1024]{2,1,0:T(8,128)(2,1)S(1)} copy(bf16[1,256,1024]{2,0,1:T(2,128)(2,1)} %bitcast.73) | data formatting | bytes 1048576
  100.7 0.9 gather_fusion
  101.6 0.2 reshape.146
  101.7 0.4 multiply_reduce_fusion
  102.1 1.9 %all_gather.15 = bf16[32,2048]{1,0:T(8,128)(2,1)S(1)} all-gather(bf16[32,1024]{1,0:T(8,128)(2,1)S(1)} %multiply_reduce_fusion), channel_id=1, replica_groups=mesh['ep'=16,'tp'=2] {'tp'}, dimensions={1}, use_global_device_ids=true | all-gather | bytes 196608 | tf_op jit(solution)/shard_map/all_gather | solution.py:115
  104.0 2.0 %all-reduce.2.cloned.1.call-done = bf16[32,2048]{1,0:T(8,128)(2,1)} async-done(((bf16[32,2048]{1,0:T(8,128)(2,1)}), bf16[32,2048]{1,0:T(8,128)(2,1)}) %all-reduce.2.cloned.1.call-update) | async-done | bytes 131088 | tf_op jit(solution)/shard_map/psum | solution.py:85
  106.1 1.1 multiply_reduce_fusion.1
  107.1 1.7 %fusion.31 = bf16[32,2048]{1,0:T(8,128)(2,1)} fusion(bf16[32,2048]{1,0:T(8,128)(2,1)S(1)} %get-tuple-element.4, bf16[32,2048]{1,0:T(8,128)(2,1)} %all-reduce.2.cloned.1.call-done, bf16[32,2048]{1,0:T(8,128)(2,1)S(1)} %all_gather.15, f32[2048]{0:T(1024)S(1)} %copy-done.12, f32[32]{0:T(128)S(1)} %add_rsqrt_fusion), kind=kLoop, calls=%fused_computation.47 | loop fusion | flops 524288 | bytes 532608 | tf_op jit(solution)/shard_map/convert_element_type | solution.py:117
  (67 shorter events, 2.1 us)
Async XLA Ops:
  7.2 4.9 %copy-start = (bf16[512,2048]{1,0:T(8,128)(2,1)S(1)}, bf16[512,2048]{1,0:T(8,128)(2,1)}, u32[]{:S(2)}) copy-start(bf16[512,2048]{1,0:T(8,128)(2,1)} %param.35) | copy-start | bytes 6291460
  7.2 4.9 %copy-start.2 = (bf16[32,2048]{1,0:T(8,128)(2,1)S(1)}, bf16[32,2048]{1,0:T(8,128)(2,1)}, u32[]{:S(2)}) copy-start(bf16[32,2048]{1,0:T(8,128)(2,1)} %param.22) | copy-start | bytes 393220
  7.2 4.9 %copy-start.11 = (f32[2048]{0:T(1024)S(1)}, f32[2048]{0:T(1024)}, u32[]{:S(2)}) copy-start(f32[2048]{0:T(1024)} %param.25) | copy-start | bytes 24580
  7.2 4.2 %copy-start.3 = (bf16[32,3,512]{2,0,1:T(8,128)(2,1)S(1)}, bf16[32,3,512]{2,0,1:T(8,128)(2,1)}, u32[]{:S(2)}) copy-start(bf16[32,3,512]{2,0,1:T(8,128)(2,1)} %param.24) | copy-start | bytes 294916
  7.2 4.2 %copy-start.17 = (bf16[4,128,128]{2,1,0:T(8,128)(2,1)S(1)}, bf16[4,128,128]{2,1,0:T(8,128)(2,1)}, u32[]{:S(2)}) copy-start(bf16[4,128,128]{2,1,0:T(8,128)(2,1)} %param.33) | copy-start | bytes 393220
  7.2 4.4 %copy-start.18 = (bf16[4,128,128]{2,1,0:T(8,128)(2,1)S(1)}, bf16[4,128,128]{2,1,0:T(8,128)(2,1)}, u32[]{:S(2)}) copy-start(bf16[4,128,128]{2,1,0:T(8,128)(2,1)} %param.32) | copy-start | bytes 393220
  7.2 4.6 %copy-start.16 = (f32[512]{0:T(512)S(1)}, f32[512]{0:T(512)}, u32[]{:S(2)}) copy-start(f32[512]{0:T(512)} %param.34) | copy-start | bytes 6148
  7.2 4.8 %copy-start.9 = (f32[32,512]{1,0:T(8,128)S(1)}, f32[32,512]{1,0:T(8,128)}, u32[]{:S(2)}) copy-start(f32[32,512]{1,0:T(8,128)} %param.23) | copy-start | bytes 196612
  7.3 43.3 %all-gather.3.cloned.1.call-start = ((), (), s32[]{:S(2)}) async-start(), calls=%async_computation.3 | async-start | bytes 1572864 | tf_op jit(solution)/shard_map/all_gather | solution.py:94
  11.4 0.6 copy-start.5
  12.1 2.6 %copy-start.7 = (f32[32,512]{1,0:T(8,128)}, f32[32,512]{1,0:T(8,128)S(1)}, u32[]{:S(2)}) copy-start(f32[32,512]{1,0:T(8,128)S(1)} %fusion.49) | copy-start | bytes 196612
  12.1 5.0 %copy-start.13 = (f32[2048]{0:T(1024)S(1)}, f32[2048]{0:T(1024)}, u32[]{:S(2)}) copy-start(f32[2048]{0:T(1024)} %param.26) | copy-start | bytes 24580
  12.2 5.2 %copy-start.14 = (s32[32,4]{0,1:T(4,128)S(1)}, s32[32,4]{0,1:T(4,128)}, u32[]{:S(2)}) copy-start(s32[32,4]{0,1:T(4,128)} %param.36) | copy-start | bytes 1540
  12.2 6.7 %copy-start.8 = (f32[2048]{0:T(1024)S(1)}, f32[2048]{0:T(1024)}, u32[]{:S(2)}) copy-start(f32[2048]{0:T(1024)} %param.27) | copy-start | bytes 24580
  43.0 23.1 %reduce-scatter.2.cloned.1.call-start = ((), (), s32[]{:S(2)}) async-start(), calls=%async_computation.4 | async-start | bytes 1572864 | tf_op jit(solution)/shard_map/reduce_scatter | solution.py:101
  50.5 2.1 %copy-start.1 = (bf16[1,256,2048]{2,1,0:T(8,128)(2,1)S(1)}, bf16[1,256,2048]{2,1,0:T(8,128)(2,1)}, u32[]{:S(2)}) copy-start(bf16[1,256,2048]{2,1,0:T(8,128)(2,1)} %all-gather.3.cloned.1.call-done) | copy-start | bytes 3145732
  75.2 22.3 %all-to-all-start.1 = ((bf16[16,2,8192]{2,1,0:T(2,128)(2,1)}), bf16[16,2,8192]{2,1,0:T(2,128)(2,1)S(1)}, u32[]{:S(2)}, u32[]{:S(2)}) async-start(bf16[16,2,8192]{2,1,0:T(2,128)(2,1)} %reshape.156), calls=%async_computation.2 | async-start | bytes 1048576 | tf_op jit(solution)/shard_map/all_to_all | solution.py:109
  82.0 4.7 %copy-start.10 = (s32[32,4]{1,0:T(8,128)S(1)}, s32[32,4]{1,0:T(8,128)}, u32[]{:S(2)}) copy-start(s32[32,4]{1,0:T(8,128)} %get-tuple-element.5) | copy-start | bytes 1540
  82.0 4.8 %copy-start.15 = (f32[32,4]{0,1:T(4,128)S(1)}, f32[32,4]{0,1:T(4,128)}, u32[]{:S(2)}) copy-start(f32[32,4]{0,1:T(4,128)} %param.37) | copy-start | bytes 1540
  82.1 4.9 %copy-start.4 = (bf16[32,3,512]{2,0,1:T(8,128)(2,1)S(1)}, bf16[32,3,512]{2,0,1:T(8,128)(2,1)}, u32[]{:S(2)}) copy-start(bf16[32,3,512]{2,0,1:T(8,128)(2,1)} %param.24) | copy-start | bytes 294916
  82.1 4.9 %copy-start.6 = (bf16[32,1,512]{2,0,1:T(8,128)(2,1)S(1)}, bf16[32,1,512]{2,0,1:T(8,128)(2,1)}, u32[]{:S(2)}) copy-start(bf16[32,1,512]{2,0,1:T(8,128)(2,1)} %copy-done.5) | copy-start | bytes 98308
  82.1 24.0 %all-reduce.2.cloned.1.call-start = ((), (), s32[]{:S(2)}) async-start(), calls=%async_computation.5 | async-start | bytes 262144 | tf_op jit(solution)/shard_map/psum | solution.py:85
  100.7 6.4 %copy-start.12 = (f32[2048]{0:T(1024)S(1)}, f32[2048]{0:T(1024)}, u32[]{:S(2)}) copy-start(f32[2048]{0:T(1024)} %param.28) | copy-start | bytes 24580
Sparse Core Ops, SparseCore 0:
  43.1 7.3 all-gather.2
  56.6 9.5 reduce-scatter.1
  86.8 19.1 all-reduce.1
